TPU v7x, 128 devices: a whole 4x4x4 slice. The times are simulated.
128 devices in a mesh: sp: 64 (over z, y, x), tp: 2 (over core).
Axes of the slice: x: 4, y: 4, z: 4, core: 2. Of those that a mesh axis runs over, the one named last changes fastest.
Arguments:
- queries: bfloat16 [8192, 1024], P('sp', 'tp'), may hold values from -6 to 6
- keys: bfloat16 [8192, 1024], P('sp', 'tp'), may hold values from -6 to 6
- values: bfloat16 [8192, 2048], P('sp', 'tp'), may hold values from -6 to 6
- out_gate: bfloat16 [8192, 2048], P('sp', 'tp'), may hold values from -6 to 6
- decay_rate: float32 [8], P('tp'), may hold values from 0 to 1
- residual: bfloat16 [8192, 2048], P(('sp', 'tp')), may hold values from -6 to 6
- out_weight: bfloat16 [2048, 2048], P('tp'), may hold values from -0.125 to 0.125
- ffn_gain: float32 [2048], replicated, may hold values from 0.1 to 1.9
- route_ids: int32 [8192, 4], P(('sp', 'tp')), may hold values from 0 to 63, all different within a row; in each aligned block of 64 rows (0 to 63, 64 to 127, ...) at most 8 rows name the same one
- route_weights: float32 [8192, 4], P(('sp', 'tp')), may hold values from 0.1 to 1
- gate_up: bfloat16 [64, 2048, 2048], P('sp', None, 'tp'), may hold values from -0.375 to 0.375
- lin_up: bfloat16 [64, 2048, 2048], P('sp', None, 'tp'), may hold values from -0.375 to 0.375
- down_weight: bfloat16 [64, 2048, 2048], P('sp', 'tp'), may hold values from -0.03125 to 0.03125
Outputs:
- layer_out: bfloat16 [8192, 2048], P(('sp', 'tp'))
Inputs may be any that keep to these rules, and one draw needn't show every extreme that they name: `route_ids`: within the rows of one device (aligned blocks of 64 rows), no expert is named by more than 8 entries, a bound that some block reaches; the 4 experts of a row differ.
All inputs are finite; a program needn't handle non-finite values.
Results may differ from a plain program's by a relative error of at most 0.03.
Values may be sent and summed in bfloat16 or wider, within the bound.
A program may use at most 128 MiB of HBM per device.

v0:
```python
import jax
import jax.numpy as jnp
from jax import lax
from jax.sharding import Mesh
from jax.sharding import PartitionSpec as P

D = 2048
DK = 128
DV = 256
SP = ("sp_0", "sp_1", "sp_2")
SP_TP = ("sp_0", "sp_1", "sp_2", "tp")
EPS = 1e-05
CLAMP_LIMIT = 7.0
SIGMOID_SLOPE = 1.702
TOP_PRECISION = lax.Precision.HIGHEST


def carried_state(state_delta, log_gamma, block_len):
    peers, mine = (lax.axis_size(SP), lax.axis_index(SP))
    heads = state_delta.shape[0]
    pieces = state_delta.astype(jnp.bfloat16).reshape(peers, -1)
    arrived = lax.all_to_all(pieces, SP, split_axis=0, concat_axis=0, tiled=True)
    own_log = lax.dynamic_index_in_dim(log_gamma, mine * heads // peers, keepdims=False)
    order = jnp.arange(peers, dtype=jnp.float32)
    gap = order[:, None] - 1.0 - order[None, :]
    weight = jnp.where(gap >= 0, jnp.exp(jnp.maximum(gap, 0.0) * block_len * own_log), 0.0)
    before = jnp.dot(weight, arrived.astype(jnp.float32), precision=TOP_PRECISION)
    returned = lax.all_to_all(
        before.astype(jnp.bfloat16), SP, split_axis=0, concat_axis=0, tiled=True
    )
    return returned.reshape(state_delta.shape).astype(jnp.float32)


def in_blocks(array, dim, peers):
    before, after = (array.shape[:dim], array.shape[dim + 1 :])
    return jnp.moveaxis(array.reshape(*before, peers, -1, *after), dim, 0)


def summed_on_arrival(array, axis, dim):
    tiles = in_blocks(array, dim, lax.axis_size(axis))
    arrived = lax.all_to_all(tiles, axis, split_axis=0, concat_axis=0, tiled=True)
    return arrived.astype(jnp.float32).sum(axis=0)


def expert_act(row_block, gate_part, lin_part):
    gate_pre = jnp.dot(row_block, gate_part, preferred_element_type=jnp.float32)
    lin_pre = jnp.dot(row_block, lin_part, preferred_element_type=jnp.float32)
    gate_clip = jnp.minimum(gate_pre, CLAMP_LIMIT)
    lin_clip = jnp.clip(lin_pre, -CLAMP_LIMIT, CLAMP_LIMIT)
    return (gate_clip * jax.nn.sigmoid(SIGMOID_SLOPE * gate_clip) * (lin_clip + 1.0)).astype(
        jnp.bfloat16
    )


def local(
    queries,
    keys,
    values,
    out_gate,
    decay_rate,
    residual,
    out_weight,
    ffn_gain,
    route_ids,
    route_weights,
    gate_up,
    lin_up,
    down_weight,
):
    block_len = queries.shape[0]
    local_heads = decay_rate.shape[0]
    log_gamma = -decay_rate
    query_heads = queries.astype(jnp.float32).reshape(block_len, local_heads, DK).transpose(1, 0, 2)
    per_head_keys = keys.astype(jnp.float32).reshape(block_len, local_heads, DK).transpose(
        1, 0, 2
    ) * DK ** (-0.5)
    per_head_values = (
        values.astype(jnp.float32).reshape(block_len, local_heads, DV).transpose(1, 0, 2)
    )
    positions = jnp.arange(block_len, dtype=jnp.float32)
    offsets = positions[:, None] - positions[None, :]
    causal = offsets >= 0
    decay_mask = jnp.where(
        causal[None], jnp.exp(jnp.where(causal, offsets, 0.0)[None] * log_gamma[:, None, None]), 0.0
    )
    trailing_decay = jnp.exp((block_len - 1.0 - positions)[None, :] * log_gamma[:, None])
    lead_decay = jnp.exp((positions + 1.0)[None, :] * log_gamma[:, None])
    attention_scores = (
        jnp.einsum("hqd,hkd->hqk", query_heads, per_head_keys, precision=TOP_PRECISION) * decay_mask
    )
    intra_block_term = jnp.einsum(
        "zfp,zpn->zfn", attention_scores, per_head_values, precision=TOP_PRECISION
    )
    state_delta = jnp.einsum(
        "mxs,mxq->msq",
        per_head_keys * trailing_decay[:, :, None],
        per_head_values,
        precision=TOP_PRECISION,
    )
    carried = carried_state(state_delta, log_gamma, block_len)
    cross_term = (
        jnp.einsum("hqd,hdv->hqv", query_heads, carried, precision=TOP_PRECISION)
        * lead_decay[:, :, None]
    )
    retained = intra_block_term + cross_term
    normed = retained * lax.rsqrt(jnp.mean(retained * retained, axis=-1, keepdims=True) + EPS)
    gated = (
        normed.transpose(1, 0, 2).reshape(block_len, local_heads * DV)
        * jax.nn.silu(out_gate.astype(jnp.float32))
    ).astype(jnp.bfloat16)
    mix_rows = summed_on_arrival(
        jnp.dot(gated, out_weight, preferred_element_type=jnp.float32).astype(jnp.bfloat16), "tp", 0
    )
    mixed = (residual.astype(jnp.float32) + mix_rows).astype(jnp.bfloat16)
    mixed_wide = mixed.astype(jnp.float32)
    normed_rows = (
        mixed_wide
        * lax.rsqrt(jnp.mean(mixed_wide * mixed_wide, axis=-1, keepdims=True) + EPS)
        * ffn_gain
    ).astype(jnp.bfloat16)
    experts = lax.axis_size(SP)
    own_rows = route_ids.shape[0]
    top_count = route_ids.shape[1]
    capacity = own_rows * top_count * lax.axis_size("tp") // experts
    flat_ids = route_ids.reshape(-1)
    one_hot = (flat_ids[:, None] == jnp.arange(experts, dtype=jnp.int32)[None, :]).astype(jnp.int32)
    slot_rank = jnp.sum(one_hot * (jnp.cumsum(one_hot, axis=0) - 1), axis=1)
    slot_index = flat_ids * capacity + slot_rank
    source_row = jnp.arange(own_rows * top_count, dtype=jnp.int32) // top_count
    slot_source = (
        jnp.full((experts * capacity,), own_rows, jnp.int32).at[slot_index].set(source_row)
    )
    padded = jnp.concatenate([normed_rows, jnp.zeros((1, D), jnp.bfloat16)], axis=0)
    outgoing = padded[slot_source].reshape(experts, capacity, D)
    gate_half = gate_up[0]
    lin_half = lin_up[0]
    down_half = down_weight[0]
    pair_rows = lax.all_gather(
        lax.all_to_all(outgoing, SP, split_axis=0, concat_axis=0, tiled=True),
        "tp",
        axis=0,
        tiled=True,
    )
    activation = expert_act(pair_rows.reshape(-1, D), gate_half, lin_half)
    partial_value = jnp.dot(activation, down_half, preferred_element_type=jnp.float32).reshape(
        pair_rows.shape
    )
    summed = summed_on_arrival(partial_value.astype(jnp.bfloat16), "tp", 0)
    returned = lax.all_to_all(
        summed.astype(jnp.bfloat16), SP, split_axis=0, concat_axis=0, tiled=True
    )
    picked = (
        returned.reshape(experts * capacity, D)[slot_index]
        .reshape(own_rows, top_count, D)
        .astype(jnp.float32)
    )
    expert_sum = jnp.sum(picked * route_weights[:, :, None], axis=1)
    return (mixed_wide + expert_sum).astype(jnp.bfloat16)


def solution(mesh):
    torus = Mesh(mesh.devices.reshape(4, 4, 4, mesh.shape["tp"]), ("sp_0", "sp_1", "sp_2", "tp"))
    in_specs = (
        P(SP, "tp"),
        P(SP, "tp"),
        P(SP, "tp"),
        P(SP, "tp"),
        P("tp"),
        P(SP_TP, None),
        P("tp", None),
        P(),
        P(SP_TP, None),
        P(SP_TP, None),
        P(SP, None, "tp"),
        P(SP, None, "tp"),
        P(SP, "tp", None),
    )
    out_specs = P(SP_TP, None)
    return jax.shard_map(local, mesh=torus, in_specs=in_specs, out_specs=out_specs, check_vma=False)
```

profile of v0, /device:TPU:0, one launch (start us, length us, event | category | flops | bytes accessed | tf_op | source)
XLA Modules:
  0.0 202.1 jit_solution(13798051839371577354)
XLA Ops:
  6.5 0.7 neg.10
  7.3 1.0 copy.102
  8.3 0.1 multiply_exponential_fusion
  8.3 1.3 convolution_convert_fusion.2
  9.7 0.1 all_to_all.35
  9.8 0.6 broadcast.223
  10.4 2.2 %reduce.4 = bf16[64,2048]{1,0:T(8,128)(2,1)S(1)} reduce(bf16[64,1,2048]{2,1,0:T(2,128)(2,1)S(1)} %all_to_all.35, bf16[]{:T(256)} %broadcast.223), dimensions={1}, to_apply=%all_to_all.35.reduce_sub_computation | reduce | bytes 524290 | tf_op jit(solution)/shard_map/all_to_all | solution.py:22
  12.6 0.9 reshape.247
  13.5 11.7 %all-to-all-start = ((bf16[64,2,1024]{2,1,0:T(2,128)(2,1)}), bf16[64,2,1024]{2,1,0:T(2,128)(2,1)S(1)}, u32[]{:S(2)}, u32[]{:S(2)}) async-start(bf16[64,2,1024]{2,1,0:T(2,128)(2,1)} %reshape.247), calls=%async_computation | async-start | bytes 524288 | tf_op jit(solution)/shard_map/all_to_all | solution.py:22
  25.2 0.1 multiply_exponential_fusion.1
  25.3 0.8 copy.90
  26.1 0.1 eq.29
  26.2 0.1 eq.25
  26.3 0.7 broadcast_multiply_fusion
  27.0 0.6 reduce-window.6
  27.6 0.2 slice_reduce_fusion
  27.8 0.1 copy.89
  27.9 0.1 mul.229
  28.0 0.1 fusion.49
  28.2 0.6 dynamic_slice.4
  29.3 1.4 scatter_custom_fusion
  30.8 5.0 %all-to-all-done = bf16[64,2,1024]{2,1,0:T(2,128)(2,1)S(1)} async-done(((bf16[64,2,1024]{2,1,0:T(2,128)(2,1)}), bf16[64,2,1024]{2,1,0:T(2,128)(2,1)S(1)}, u32[]{:S(2)}, u32[]{:S(2)}) %all-to-all-start) | async-done | bytes 262176 | tf_op jit(solution)/shard_map/all_to_all | solution.py:22
  35.8 0.2 reshape.248
  36.0 0.5 fusion.11
  36.5 0.8 reduce.5
  37.3 0.9 reshape.249
  38.2 5.4 %all-to-all-start.1 = ((bf16[64,2,1024]{2,1,0:T(2,128)(2,1)}), bf16[64,2,1024]{2,1,0:T(2,128)(2,1)S(1)}, u32[]{:S(2)}, u32[]{:S(2)}) async-start(bf16[64,2,1024]{2,1,0:T(2,128)(2,1)} %reshape.249), calls=%async_computation.1 | async-start | bytes 524288 | tf_op jit(solution)/shard_map/all_to_all | solution.py:28
  43.5 0.0 all-gather.2.cloned.1.call-start
  43.6 0.2 copy.88
  43.8 0.4 fusion.22
  44.2 10.0 %all-to-all-done.1 = bf16[64,2,1024]{2,1,0:T(2,128)(2,1)S(1)} async-done(((bf16[64,2,1024]{2,1,0:T(2,128)(2,1)}), bf16[64,2,1024]{2,1,0:T(2,128)(2,1)S(1)}, u32[]{:S(2)}, u32[]{:S(2)}) %all-to-all-start.1) | async-done | bytes 262176 | tf_op jit(solution)/shard_map/all_to_all | solution.py:28
  54.2 0.2 reshape.250
  54.4 1.5 reduce.1
  55.9 0.1 reshape.207
  56.0 0.2 fusion.43
  56.3 0.5 fusion.32
  56.8 0.2 fusion.34
  57.0 0.2 copy.87
  57.2 0.0 copy-start.3
  57.2 0.1 fusion.35
  57.4 2.9 %convolution_convert_fusion = bf16[128,2048]{1,0:T(8,128)(2,1)S(1)} fusion(bf16[128,1024]{0,1:T(8,128)(2,1)S(1)} %fusion.35, bf16[1024,2048]{1,0:T(8,128)(2,1)} %param.19), kind=kOutput, calls=%fused_computation.13 | convolution fusion | flops 537133056 | bytes 4980736 | tf_op jit(solution)/shard_map/dot_general | solution.py:112
  60.3 4.2 %all_to_all.42 = bf16[2,64,2048]{2,1,0:T(8,128)(2,1)S(1)} all-to-all(bf16[2,64,2048]{2,1,0:T(8,128)(2,1)S(1)} %bitcast.118), channel_id=1, replica_groups=mesh['sp_0'=4,'sp_1'=4,'sp_2'=4,'tp'=2] {'tp'}, dimensions={0} | all-to-all | bytes 1048576 | tf_op jit(solution)/shard_map/all_to_all | solution.py:41
  64.5 0.1 convert_reduce_fusion
  64.6 0.2 fusion.27
  64.8 0.1 fusion.29
  65.0 2.5 %gather_fusion = bf16[512,2048]{1,0:T(8,128)(2,1)S(1)} fusion(bf16[65,2048]{1,0:T(8,128)(2,1)S(1)} %concatenate.3, s32[1024]{0:T(1024)S(1)} %pad_clamp_fusion.1), kind=kCustom, calls=%fused_computation | custom fusion | bytes 4196352 | tf_op jit(solution)/shard_map/gather | solution.py:134
  67.4 35.2 %all_to_all.43 = bf16[64,8,2048]{2,1,0:T(8,128)(2,1)} all-to-all(bf16[64,8,2048]{2,1,0:T(8,128)(2,1)S(1)} %bitcast.114), channel_id=1, replica_groups=mesh['sp_0'=4,'sp_1'=4,'sp_2'=4,'tp'=2] {'sp_0','sp_1','sp_2'}, dimensions={0} | all-to-all | bytes 4194304 | tf_op jit(solution)/shard_map/all_to_all | solution.py:139
  102.7 0.0 all-gather.2.cloned.1.call-update
  102.7 13.1 %all-gather.2.cloned.1.call-done = bf16[128,8,2048]{2,1,0:T(8,128)(2,1)} async-done(((bf16[64,8,2048]{2,1,0:T(8,128)(2,1)}), bf16[128,8,2048]{2,1,0:T(8,128)(2,1)}) %all-gather.2.cloned.1.call-update) | async-done | bytes 4194320 | tf_op jit(solution)/shard_map/all_gather | solution.py:138
  115.8 7.6 %fusion.2 = f32[1024,1024]{1,0:T(8,128)S(1)} fusion(bf16[1,2048,1024]{2,1,0:T(8,128)(2,1)} %param.24, bf16[128,8,2048]{2,1,0:T(8,128)(2,1)} %all-gather.2.cloned.1.call-done), kind=kOutput, calls=%fused_computation.5 | convolution fusion | flops 4294967296 | bytes 12582912 | tf_op jit(solution)/shard_map/dot_general | solution.py:47
  123.5 5.8 %fusion.17 = bf16[128,8,1024]{2,1,0:T(8,128)(2,1)S(1)} fusion(f32[1024,1024]{1,0:T(8,128)S(1)} %fusion.2, bf16[1,2048,1024]{2,1,0:T(8,128)(2,1)S(1)} %copy-done.6, bf16[128,8,2048]{2,1,0:T(8,128)(2,1)S(1)} %copy-done.8), kind=kOutput, calls=%fused_computation.18 | convolution fusion | flops 4305453056 | bytes 14680064 | tf_op jit(solution)/shard_map/dot_general | solution.py:46
  129.3 5.2 %fusion.8 = bf16[128,8,2048]{2,0,1:T(8,128)(2,1)S(1)} fusion(bf16[1,1024,2048]{2,1,0:T(8,128)(2,1)S(1)} %copy-done.7, bf16[128,8,1024]{2,1,0:T(8,128)(2,1)S(1)} %fusion.17), kind=kOutput, calls=%fused_computation.12 | convolution fusion | flops 4297064448 | bytes 10485760 | tf_op jit(solution)/shard_map/dot_general | solution.py:145
  134.5 0.6 copy.94
  135.1 8.2 %all_to_all.44 = bf16[2,64,8,2048]{3,1,2,0:T(8,128)(2,1)} all-to-all(bf16[2,64,8,2048]{3,1,2,0:T(8,128)(2,1)S(1)} %copy.94), channel_id=1, replica_groups=mesh['sp_0'=4,'sp_1'=4,'sp_2'=4,'tp'=2] {'tp'}, dimensions={0} | all-to-all | bytes 8388608 | tf_op jit(solution)/shard_map/all_to_all | solution.py:41
  143.2 3.5 %reduce_sum.64 = bf16[64,8,2048]{2,0,1:T(8,128)(2,1)S(1)} reduce(bf16[2,64,8,2048]{3,1,2,0:T(8,128)(2,1)} %all_to_all.44, bf16[]{:T(256)} %constant.96.clone.1), dimensions={0}, to_apply=%region_7.8 | reduce | flops 1048576 | bytes 6291458 | tf_op jit(solution)/shard_map/reduce_sum | solution.py:42
  146.7 0.0 copy-start.5
  146.7 2.5 %copy.96 = bf16[64,8,2048]{2,1,0:T(8,128)(2,1)} copy(bf16[64,8,2048]{2,0,1:T(8,128)(2,1)S(1)} %reduce_sum.64) | data formatting | bytes 4194304 | tf_op jit(solution)/shard_map/reduce_sum | solution.py:42
  149.2 10.6 %all-to-all-start.5 = ((bf16[64,8,2048]{2,1,0:T(8,128)(2,1)}), bf16[64,8,2048]{2,1,0:T(8,128)(2,1)S(1)}, u32[]{:S(2)}, u32[]{:S(2)}) async-start(bf16[64,8,2048]{2,1,0:T(8,128)(2,1)} %copy.96), calls=%async_computation.5 | async-start | bytes 4194304 | tf_op jit(solution)/shard_map/all_to_all | solution.py:149
  159.9 0.7 copy.97
  160.6 29.4 %all-to-all-done.5 = bf16[64,8,2048]{2,1,0:T(8,128)(2,1)S(1)} async-done(((bf16[64,8,2048]{2,1,0:T(8,128)(2,1)}), bf16[64,8,2048]{2,1,0:T(8,128)(2,1)S(1)}, u32[]{:S(2)}, u32[]{:S(2)}) %all-to-all-start.5) | async-done | bytes 2097184 | tf_op jit(solution)/shard_map/all_to_all | solution.py:149
  190.0 1.4 gather_fusion.1
  191.4 0.7 reshape.215
  192.1 2.4 %multiply_reduce_fusion = f32[64,2048]{1,0:T(8,128)S(1)} fusion(f32[64,4,2048]{2,1,0:T(4,128)S(1)} %reshape.215, f32[64,4]{1,0:T(8,128)} %copy.97), kind=kLoop, calls=%fused_computation.17 | loop fusion | flops 917504 | bytes 2622464 | tf_op jit(solution)/shard_map/reduce_sum | solution.py:157
  194.5 0.8 fusion.30
  (31 shorter events, 0.2 us)
Async XLA Ops:
  6.5 37.3 %copy-start = (bf16[128,512]{1,0:T(8,128)(2,1)S(1)}, bf16[128,512]{1,0:T(8,128)(2,1)}, u32[]{:S(2)}) copy-start(bf16[128,512]{1,0:T(8,128)(2,1)} %param.13) | copy-start | bytes 393220
  6.5 37.1 %copy-start.2 = (bf16[128,1024]{1,0:T(8,128)(2,1)S(1)}, bf16[128,1024]{1,0:T(8,128)(2,1)}, u32[]{:S(2)}) copy-start(bf16[128,1024]{1,0:T(8,128)(2,1)} %param.16) | copy-start | bytes 786436
  13.5 42.8 %copy-start.1 = (bf16[128,1024]{1,0:T(8,128)(2,1)S(1)}, bf16[128,1024]{1,0:T(8,128)(2,1)}, u32[]{:S(2)}) copy-start(bf16[128,1024]{1,0:T(8,128)(2,1)} %param.15) | copy-start | bytes 786436
  13.5 22.3 %all-to-all-start = ((bf16[64,2,1024]{2,1,0:T(2,128)(2,1)}), bf16[64,2,1024]{2,1,0:T(2,128)(2,1)S(1)}, u32[]{:S(2)}, u32[]{:S(2)}) async-start(bf16[64,2,1024]{2,1,0:T(2,128)(2,1)} %reshape.247), calls=%async_computation | async-start | bytes 524288 | tf_op jit(solution)/shard_map/all_to_all | solution.py:22
  38.2 16.0 %all-to-all-start.1 = ((bf16[64,2,1024]{2,1,0:T(2,128)(2,1)}), bf16[64,2,1024]{2,1,0:T(2,128)(2,1)S(1)}, u32[]{:S(2)}, u32[]{:S(2)}) async-start(bf16[64,2,1024]{2,1,0:T(2,128)(2,1)} %reshape.249), calls=%async_computation.1 | async-start | bytes 524288 | tf_op jit(solution)/shard_map/all_to_all | solution.py:28
  43.5 72.3 %all-gather.2.cloned.1.call-start = ((), (), s32[]{:S(2)}) async-start(), calls=%async_computation.6 | async-start | bytes 6291456 | tf_op jit(solution)/shard_map/all_gather | solution.py:138
  57.2 7.4 %copy-start.3 = (bf16[64,2048]{1,0:T(8,128)(2,1)S(1)}, bf16[64,2048]{1,0:T(8,128)(2,1)}, u32[]{:S(2)}) copy-start(bf16[64,2048]{1,0:T(8,128)(2,1)} %param.18) | copy-start | bytes 786436
  57.4 7.4 %copy-start.4 = (f32[2048]{0:T(1024)S(1)}, f32[2048]{0:T(1024)}, u32[]{:S(2)}) copy-start(f32[2048]{0:T(1024)} %param.20) | copy-start | bytes 24580
  115.8 7.7 %copy-start.6 = (bf16[1,2048,1024]{2,1,0:T(8,128)(2,1)S(1)}, bf16[1,2048,1024]{2,1,0:T(8,128)(2,1)}, u32[]{:S(2)}) copy-start(bf16[1,2048,1024]{2,1,0:T(8,128)(2,1)} %param.23) | copy-start | bytes 12582916
  115.8 7.7 %copy-start.8 = (bf16[128,8,2048]{2,1,0:T(8,128)(2,1)S(1)}, bf16[128,8,2048]{2,1,0:T(8,128)(2,1)}, u32[]{:S(2)}) copy-start(bf16[128,8,2048]{2,1,0:T(8,128)(2,1)} %all-gather.2.cloned.1.call-done) | copy-start | bytes 12582916
  123.5 5.8 %copy-start.7 = (bf16[1,1024,2048]{2,1,0:T(8,128)(2,1)S(1)}, bf16[1,1024,2048]{2,1,0:T(8,128)(2,1)}, u32[]{:S(2)}) copy-start(bf16[1,1024,2048]{2,1,0:T(8,128)(2,1)} %param.25) | copy-start | bytes 12582916
  146.7 13.1 %copy-start.5 = (f32[64,4]{0,1:T(4,128)S(1)}, f32[64,4]{0,1:T(4,128)}, u32[]{:S(2)}) copy-start(f32[64,4]{0,1:T(4,128)} %param.22) | copy-start | bytes 3076
  149.2 40.8 %all-to-all-start.5 = ((bf16[64,8,2048]{2,1,0:T(8,128)(2,1)}), bf16[64,8,2048]{2,1,0:T(8,128)(2,1)S(1)}, u32[]{:S(2)}, u32[]{:S(2)}) async-start(bf16[64,8,2048]{2,1,0:T(8,128)(2,1)} %copy.96), calls=%async_computation.5 | async-start | bytes 4194304 | tf_op jit(solution)/shard_map/all_to_all | solution.py:149
Sparse Core Ops, SparseCore 0:
  102.8 12.9 all-gather.1
where the time goes:
time: 203 us; the launch traced here: 202 us
  waiting for transfers between devices  57.5 us (28%)
  blocking collectives  47.6 us (23%)
  starting transfers between devices  27.7 us (14%)
  matrix products  24.4 us (12%)
  local copies, waits for them, and re-layouts  16.2 us (8%)
  between operations  14.4 us (7%)
  other arithmetic  14.3 us (7%)
    all_to_all x1, blocking collectives, local(): lax.all_to_all(outgoing, SP, split_axis=0, concat_axis=0, tiled=True)  35.2 us
    all_to_all x1, waiting for transfers between devices, local(): lax.all_to_all(summed.astype(jnp.bfloat16), SP, split_axis=0, concat_axis...  29.4 us
    all_gather x1, waiting for transfers between devices, local(): lax.all_gather(lax.all_to_all(outgoing, SP, split_axis=0, concat_axis=0,...  13.1 us
    all_to_all x2, blocking collectives, summed_on_arrival(): lax.all_to_all(tiles, axis, split_axis=0, concat_axis=0, tiled=True)  12.3 us
    all_to_all x1, starting transfers between devices, carried_state(): lax.all_to_all(pieces, SP, split_axis=0, concat_axis=0, tiled=True)  11.7 us
    all_to_all x1, starting transfers between devices, local(): lax.all_to_all(summed.astype(jnp.bfloat16), SP, split_axis=0, concat_axis...  10.6 us
    all_to_all x1, waiting for transfers between devices, carried_state(): lax.all_to_all(before.astype(jnp.bfloat16), SP, split_axis=0, concat_axis...  9.95 us
    dot_general x1, matrix products, expert_act(): lin_pre = jnp.dot(row_block, lin_part, preferred_element_type=jnp.float32)  7.65 us
  transfers between devices with their start and end apart: 4, of which 4 were waited for; matrix products, arithmetic and copies ran while one was open for 3% of the time, Pallas kernels for 0%

commit v1 on v0

--- a/solution.py
+++ b/solution.py
@@ -135,11 +135,18 @@
     gate_half = gate_up[0]
     lin_half = lin_up[0]
     down_half = down_weight[0]
-    pair_rows = lax.all_gather(
-        lax.all_to_all(outgoing, SP, split_axis=0, concat_axis=0, tiled=True),
-        "tp",
+    pair_rows = jnp.concatenate(
+        lax.all_to_all(
+            jnp.stack(
+                lax.axis_size("tp")
+                * [lax.all_to_all(outgoing, SP, split_axis=0, concat_axis=0, tiled=True)],
+                axis=0,
+            ),
+            axis_name="tp",
+            split_axis=0,
+            concat_axis=0,
+        ),
         axis=0,
-        tiled=True,
     )
     activation = expert_act(pair_rows.reshape(-1, D), gate_half, lin_half)
     partial_value = jnp.dot(activation, down_half, preferred_element_type=jnp.float32).reshape(

time: 203 us -> 176 us (0.87)
  between operations: 14.4 us -> 1.02 us
  waiting for transfers between devices: 57.5 us -> 44.8 us
  blocking collectives: 47.6 us -> 54.8 us
  starting transfers between devices: 27.7 us -> 22.7 us
  matrix products: 24.4 us -> 21.3 us
    all_gather x1 -> x0, waiting for transfers between devices: 13.1 us -> none  [local(): lax.all_gather(lax.all_to_all(outgoing, SP, split_axis=0, concat_axis=0,...]
    all_to_all x0 -> x1, blocking collectives: none -> 7.37 us  [local(): lax.all_to_all(jnp.stack(lax.axis_size('tp') * [lax.all_to_all(outgoing,...]
    all_to_all x1, starting transfers between devices: 10.6 us -> 5.67 us  [local(): lax.all_to_all(summed.astype(jnp.bfloat16), SP, split_axis=0, concat_axis...]
    dot_general x1, matrix products: 7.65 us -> 4.53 us  [expert_act(): lin_pre = jnp.dot(row_block, lin_part, preferred_element_type=jnp.float32)]
  transfers between devices with their start and end apart: 4 -> 3, of which waited for: 4 -> 3; matrix products, arithmetic and copies ran while one was open for 3% -> 4% of each run, Pallas kernels for 0% -> 0%
where the time goes in v1:
time: 176 us; the launch traced here: 175 us
  blocking collectives  54.8 us (31%)
  waiting for transfers between devices  44.8 us (25%)
  starting transfers between devices  22.7 us (13%)
  matrix products  21.3 us (12%)
  local copies, waits for them, and re-layouts  16.2 us (9%)
  other arithmetic  14.6 us (8%)
    all_to_all x1, blocking collectives, local(): lax.all_to_all(outgoing, SP, split_axis=0, concat_axis=0, tiled=True)  35.1 us
    all_to_all x1, waiting for transfers between devices, local(): lax.all_to_all(summed.astype(jnp.bfloat16), SP, split_axis=0, concat_axis...  29.8 us
    all_to_all x2, blocking collectives, summed_on_arrival(): lax.all_to_all(tiles, axis, split_axis=0, concat_axis=0, tiled=True)  12.3 us
    all_to_all x1, starting transfers between devices, carried_state(): lax.all_to_all(pieces, SP, split_axis=0, concat_axis=0, tiled=True)  11.7 us
    all_to_all x1, waiting for transfers between devices, carried_state(): lax.all_to_all(before.astype(jnp.bfloat16), SP, split_axis=0, concat_axis...  10 us
    all_to_all x1, blocking collectives, local(): lax.all_to_all(jnp.stack(lax.axis_size('tp') * [lax.all_to_all(outgoing,...  7.37 us
    dot_general x1, matrix products, expert_act(): gate_pre = jnp.dot(row_block, gate_part, preferred_element_type=jnp.float32)  5.76 us
    all_to_all x1, starting transfers between devices, local(): lax.all_to_all(summed.astype(jnp.bfloat16), SP, split_axis=0, concat_axis...  5.67 us
  transfers between devices with their start and end apart: 3, of which 3 were waited for; matrix products, arithmetic and copies ran while one was open for 4% of the time, Pallas kernels for 0%

profile of v1, /device:TPU:0, one launch (start us, length us, event | category | flops | bytes accessed | tf_op | source)
XLA Modules:
  0.0 175.4 jit_solution(14057252559338758177)
XLA Ops:
  0.0 0.7 neg.10
  0.7 1.0 copy.102
  1.7 0.1 multiply_exponential_fusion
  1.8 1.3 convolution_convert_fusion.2
  3.1 0.1 all_to_all.39
  3.3 0.6 broadcast.223
  3.9 2.2 %reduce.4 = bf16[64,2048]{1,0:T(8,128)(2,1)S(1)} reduce(bf16[64,1,2048]{2,1,0:T(2,128)(2,1)S(1)} %all_to_all.39, bf16[]{:T(256)} %broadcast.223), dimensions={1}, to_apply=%all_to_all.39.reduce_sub_computation | reduce | bytes 524290 | tf_op jit(solution)/shard_map/all_to_all | solution.py:22
  6.1 0.9 reshape.243
  7.0 11.7 %all-to-all-start = ((bf16[64,2,1024]{2,1,0:T(2,128)(2,1)}), bf16[64,2,1024]{2,1,0:T(2,128)(2,1)S(1)}, u32[]{:S(2)}, u32[]{:S(2)}) async-start(bf16[64,2,1024]{2,1,0:T(2,128)(2,1)} %reshape.243), calls=%async_computation | async-start | bytes 524288 | tf_op jit(solution)/shard_map/all_to_all | solution.py:22
  18.7 0.1 multiply_exponential_fusion.1
  18.8 0.8 copy.90
  19.5 0.1 eq.29
  19.6 0.1 eq.25
  19.8 0.7 broadcast_multiply_fusion
  20.5 0.6 reduce-window.6
  21.1 0.2 slice_reduce_fusion
  21.3 0.1 copy.89
  21.4 0.1 mul.229
  21.5 0.1 fusion.43
  21.7 0.6 dynamic_slice.4
  22.8 1.4 scatter_custom_fusion
  24.2 5.0 %all-to-all-done = bf16[64,2,1024]{2,1,0:T(2,128)(2,1)S(1)} async-done(((bf16[64,2,1024]{2,1,0:T(2,128)(2,1)}), bf16[64,2,1024]{2,1,0:T(2,128)(2,1)S(1)}, u32[]{:S(2)}, u32[]{:S(2)}) %all-to-all-start) | async-done | bytes 262176 | tf_op jit(solution)/shard_map/all_to_all | solution.py:22
  29.2 0.2 reshape.244
  29.5 0.5 fusion.9
  29.9 0.8 reduce.5
  30.8 0.9 reshape.245
  31.6 5.4 %all-to-all-start.1 = ((bf16[64,2,1024]{2,1,0:T(2,128)(2,1)}), bf16[64,2,1024]{2,1,0:T(2,128)(2,1)S(1)}, u32[]{:S(2)}, u32[]{:S(2)}) async-start(bf16[64,2,1024]{2,1,0:T(2,128)(2,1)} %reshape.245), calls=%async_computation.1 | async-start | bytes 524288 | tf_op jit(solution)/shard_map/all_to_all | solution.py:28
  37.0 0.2 copy.88
  37.2 0.4 fusion.16
  37.6 10.0 %all-to-all-done.1 = bf16[64,2,1024]{2,1,0:T(2,128)(2,1)S(1)} async-done(((bf16[64,2,1024]{2,1,0:T(2,128)(2,1)}), bf16[64,2,1024]{2,1,0:T(2,128)(2,1)S(1)}, u32[]{:S(2)}, u32[]{:S(2)}) %all-to-all-start.1) | async-done | bytes 262176 | tf_op jit(solution)/shard_map/all_to_all | solution.py:28
  47.6 0.2 reshape.246
  47.8 1.5 reduce.1
  49.4 0.1 reshape.204
  49.5 0.2 fusion.37
  49.7 0.5 fusion.26
  50.3 0.2 fusion.28
  50.5 0.2 copy.87
  50.7 0.0 copy-start.4
  50.7 0.1 fusion.29
  50.9 0.0 copy-start.5
  50.9 2.9 %convolution_convert_fusion = bf16[128,2048]{1,0:T(8,128)(2,1)S(1)} fusion(bf16[128,1024]{0,1:T(8,128)(2,1)S(1)} %fusion.29, bf16[1024,2048]{1,0:T(8,128)(2,1)} %param.19), kind=kOutput, calls=%fused_computation.12 | convolution fusion | flops 537133056 | bytes 4980736 | tf_op jit(solution)/shard_map/dot_general | solution.py:112
  53.8 4.2 %all_to_all.47 = bf16[2,64,2048]{2,1,0:T(8,128)(2,1)S(1)} all-to-all(bf16[2,64,2048]{2,1,0:T(8,128)(2,1)S(1)} %bitcast.116), channel_id=1, replica_groups=mesh['sp_0'=4,'sp_1'=4,'sp_2'=4,'tp'=2] {'tp'}, dimensions={0} | all-to-all | bytes 1048576 | tf_op jit(solution)/shard_map/all_to_all | solution.py:41
  58.0 0.1 convert_reduce_fusion
  58.1 0.2 fusion.21
  58.3 0.1 fusion.23
  58.4 2.5 %gather_fusion = bf16[512,2048]{1,0:T(8,128)(2,1)S(1)} fusion(bf16[65,2048]{1,0:T(8,128)(2,1)S(1)} %concatenate.3, s32[1024]{0:T(1024)S(1)} %pad_clamp_fusion.1), kind=kCustom, calls=%fused_computation | custom fusion | bytes 4196352 | tf_op jit(solution)/shard_map/gather | solution.py:134
  60.9 35.1 %all_to_all.48 = bf16[64,8,2048]{2,1,0:T(8,128)(2,1)S(1)} all-to-all(bf16[64,8,2048]{2,1,0:T(8,128)(2,1)S(1)} %bitcast.109), channel_id=1, replica_groups=mesh['sp_0'=4,'sp_1'=4,'sp_2'=4,'tp'=2] {'sp_0','sp_1','sp_2'}, dimensions={0} | all-to-all | bytes 4194304 | tf_op jit(solution)/shard_map/all_to_all | solution.py:142
  96.0 0.4 pad_maximum_fusion
  96.4 0.0 copy-start.7
  96.4 7.4 %all_to_all.49 = bf16[2,64,8,2048]{3,2,1,0:T(8,128)(2,1)S(1)} all-to-all(bf16[2,64,8,2048]{3,2,1,0:T(8,128)(2,1)S(1)} %pad_maximum_fusion), channel_id=1, replica_groups=mesh['sp_0'=4,'sp_1'=4,'sp_2'=4,'tp'=2] {'tp'}, dimensions={0} | all-to-all | bytes 8388608 | tf_op jit(solution)/shard_map/all_to_all | solution.py:139
  103.8 4.5 %fusion.2 = f32[1024,1024]{1,0:T(8,128)S(1)} fusion(bf16[1024,2048]{1,0:T(8,128)(2,1)S(1)} %bitcast.111, bf16[1,2048,1024]{2,1,0:T(8,128)(2,1)S(1)} %copy-done.7), kind=kOutput, calls=%fused_computation.6 | convolution fusion | flops 4294967296 | bytes 12582912 | tf_op jit(solution)/shard_map/dot_general | solution.py:47
  108.3 5.8 %fusion.13 = bf16[128,8,1024]{2,1,0:T(8,128)(2,1)S(1)} fusion(f32[1024,1024]{1,0:T(8,128)S(1)} %fusion.2, bf16[1024,2048]{1,0:T(8,128)(2,1)S(1)} %bitcast.112, bf16[1,2048,1024]{2,1,0:T(8,128)(2,1)S(1)} %copy-done.8), kind=kOutput, calls=%fused_computation.17 | convolution fusion | flops 4305453056 | bytes 14680064 | tf_op jit(solution)/shard_map/dot_general | solution.py:46
  114.1 5.2 %fusion.6 = bf16[128,8,2048]{2,0,1:T(8,128)(2,1)S(1)} fusion(bf16[1,1024,2048]{2,1,0:T(8,128)(2,1)S(1)} %copy-done.9, bf16[128,8,1024]{2,1,0:T(8,128)(2,1)S(1)} %fusion.13), kind=kOutput, calls=%fused_computation.11 | convolution fusion | flops 4297064448 | bytes 10485760 | tf_op jit(solution)/shard_map/dot_general | solution.py:152
  119.3 0.6 copy.94
  119.9 8.2 %all_to_all.50 = bf16[2,64,8,2048]{3,1,2,0:T(8,128)(2,1)} all-to-all(bf16[2,64,8,2048]{3,1,2,0:T(8,128)(2,1)S(1)} %copy.94), channel_id=1, replica_groups=mesh['sp_0'=4,'sp_1'=4,'sp_2'=4,'tp'=2] {'tp'}, dimensions={0} | all-to-all | bytes 8388608 | tf_op jit(solution)/shard_map/all_to_all | solution.py:41
  128.0 3.5 %reduce_sum.64 = bf16[64,8,2048]{2,0,1:T(8,128)(2,1)S(1)} reduce(bf16[2,64,8,2048]{3,1,2,0:T(8,128)(2,1)} %all_to_all.50, bf16[]{:T(256)} %constant.96.clone.1), dimensions={0}, to_apply=%region_7.8 | reduce | flops 1048576 | bytes 6291458 | tf_op jit(solution)/shard_map/reduce_sum | solution.py:42
  131.5 2.5 %copy.96 = bf16[64,8,2048]{2,1,0:T(8,128)(2,1)} copy(bf16[64,8,2048]{2,0,1:T(8,128)(2,1)S(1)} %reduce_sum.64) | data formatting | bytes 4194304 | tf_op jit(solution)/shard_map/reduce_sum | solution.py:42
  134.0 5.7 %all-to-all-start.6 = ((bf16[64,8,2048]{2,1,0:T(8,128)(2,1)}), bf16[64,8,2048]{2,1,0:T(8,128)(2,1)S(1)}, u32[]{:S(2)}, u32[]{:S(2)}) async-start(bf16[64,8,2048]{2,1,0:T(8,128)(2,1)} %copy.96), calls=%async_computation.6 | async-start | bytes 4194304 | tf_op jit(solution)/shard_map/all_to_all | solution.py:156
  139.7 0.7 copy.97
  140.4 29.8 %all-to-all-done.6 = bf16[64,8,2048]{2,1,0:T(8,128)(2,1)S(1)} async-done(((bf16[64,8,2048]{2,1,0:T(8,128)(2,1)}), bf16[64,8,2048]{2,1,0:T(8,128)(2,1)S(1)}, u32[]{:S(2)}, u32[]{:S(2)}) %all-to-all-start.6) | async-done | bytes 2097184 | tf_op jit(solution)/shard_map/all_to_all | solution.py:156
  170.2 1.4 gather_fusion.1
  171.6 0.7 reshape.211
  172.3 2.3 %multiply_reduce_fusion = f32[64,2048]{1,0:T(8,128)S(1)} fusion(f32[64,4,2048]{2,1,0:T(4,128)S(1)} %reshape.211, f32[64,4]{1,0:T(8,128)} %copy.97), kind=kLoop, calls=%fused_computation.16 | loop fusion | flops 917504 | bytes 2622464 | tf_op jit(solution)/shard_map/reduce_sum | solution.py:164
  174.6 0.8 fusion.24
  (32 shorter events, 0.2 us)
Async XLA Ops:
  0.0 37.2 %copy-start = (bf16[128,512]{1,0:T(8,128)(2,1)S(1)}, bf16[128,512]{1,0:T(8,128)(2,1)}, u32[]{:S(2)}) copy-start(bf16[128,512]{1,0:T(8,128)(2,1)} %param.13) | copy-start | bytes 393220
  0.0 37.0 %copy-start.3 = (bf16[128,1024]{1,0:T(8,128)(2,1)S(1)}, bf16[128,1024]{1,0:T(8,128)(2,1)}, u32[]{:S(2)}) copy-start(bf16[128,1024]{1,0:T(8,128)(2,1)} %param.16) | copy-start | bytes 786436
  7.0 42.8 %copy-start.2 = (bf16[128,1024]{1,0:T(8,128)(2,1)S(1)}, bf16[128,1024]{1,0:T(8,128)(2,1)}, u32[]{:S(2)}) copy-start(bf16[128,1024]{1,0:T(8,128)(2,1)} %param.15) | copy-start | bytes 786436
  7.0 22.3 %all-to-all-start = ((bf16[64,2,1024]{2,1,0:T(2,128)(2,1)}), bf16[64,2,1024]{2,1,0:T(2,128)(2,1)S(1)}, u32[]{:S(2)}, u32[]{:S(2)}) async-start(bf16[64,2,1024]{2,1,0:T(2,128)(2,1)} %reshape.243), calls=%async_computation | async-start | bytes 524288 | tf_op jit(solution)/shard_map/all_to_all | solution.py:22
  31.6 16.0 %all-to-all-start.1 = ((bf16[64,2,1024]{2,1,0:T(2,128)(2,1)}), bf16[64,2,1024]{2,1,0:T(2,128)(2,1)S(1)}, u32[]{:S(2)}, u32[]{:S(2)}) async-start(bf16[64,2,1024]{2,1,0:T(2,128)(2,1)} %reshape.245), calls=%async_computation.1 | async-start | bytes 524288 | tf_op jit(solution)/shard_map/all_to_all | solution.py:28
  50.7 7.4 %copy-start.4 = (bf16[64,2048]{1,0:T(8,128)(2,1)S(1)}, bf16[64,2048]{1,0:T(8,128)(2,1)}, u32[]{:S(2)}) copy-start(bf16[64,2048]{1,0:T(8,128)(2,1)} %param.18) | copy-start | bytes 786436
  50.9 7.4 %copy-start.5 = (f32[2048]{0:T(1024)S(1)}, f32[2048]{0:T(1024)}, u32[]{:S(2)}) copy-start(f32[2048]{0:T(1024)} %param.20) | copy-start | bytes 24580
  96.4 7.4 %copy-start.7 = (bf16[1,2048,1024]{2,1,0:T(8,128)(2,1)S(1)}, bf16[1,2048,1024]{2,1,0:T(8,128)(2,1)}, u32[]{:S(2)}) copy-start(bf16[1,2048,1024]{2,1,0:T(8,128)(2,1)} %param.24) | copy-start | bytes 12582916
  103.8 4.5 %copy-start.8 = (bf16[1,2048,1024]{2,1,0:T(8,128)(2,1)S(1)}, bf16[1,2048,1024]{2,1,0:T(8,128)(2,1)}, u32[]{:S(2)}) copy-start(bf16[1,2048,1024]{2,1,0:T(8,128)(2,1)} %param.23) | copy-start | bytes 12582916
  108.3 5.8 %copy-start.9 = (bf16[1,1024,2048]{2,1,0:T(8,128)(2,1)S(1)}, bf16[1,1024,2048]{2,1,0:T(8,128)(2,1)}, u32[]{:S(2)}) copy-start(bf16[1,1024,2048]{2,1,0:T(8,128)(2,1)} %param.25) | copy-start | bytes 12582916
  131.5 8.2 %copy-start.6 = (f32[64,4]{0,1:T(4,128)S(1)}, f32[64,4]{0,1:T(4,128)}, u32[]{:S(2)}) copy-start(f32[64,4]{0,1:T(4,128)} %param.22) | copy-start | bytes 3076
  134.0 36.2 %all-to-all-start.6 = ((bf16[64,8,2048]{2,1,0:T(8,128)(2,1)}), bf16[64,8,2048]{2,1,0:T(8,128)(2,1)S(1)}, u32[]{:S(2)}, u32[]{:S(2)}) async-start(bf16[64,8,2048]{2,1,0:T(8,128)(2,1)} %copy.96), calls=%async_computation.6 | async-start | bytes 4194304 | tf_op jit(solution)/shard_map/all_to_all | solution.py:156
  170.2 5.2 %copy-start.1 = (bf16[128,512]{1,0:T(8,128)(2,1)S(1)}, bf16[128,512]{1,0:T(8,128)(2,1)}, u32[]{:S(2)}) copy-start(bf16[128,512]{1,0:T(8,128)(2,1)} %param.13) | copy-start | bytes 393220
